TPU v7x, 256 devices: a whole 4x4x8 slice. The times are simulated.
256 devices in a mesh: ep: 64 (over z, x, core), tp: 4 (over y).
Axes of the slice: x: 4, y: 4, z: 8, core: 2. Of those that a mesh axis runs over, the one named last changes fastest.
Arguments:
- tokens: bfloat16 [16384, 2048], P('ep'), may hold values from -6 to 6
- norm_gain: float32 [2048], replicated, may hold values from 0.1 to 1.9
- expert_ids: int32 [16384, 4], P('ep'), may hold values from 0 to 63, all different within a row; in each aligned block of 256 rows (0 to 255, 256 to 511, ...) at most 32 rows name the same one
- route_weights: float32 [16384, 4], P('ep'), may hold values from 0.05 to 1
- gate_weight: bfloat16 [64, 2048, 2048], P('ep', None, 'tp'), as said below
- up_weight: bfloat16 [64, 2048, 2048], P('ep', None, 'tp'), as said below
- down_weight: bfloat16 [64, 2048, 2048], P('ep', 'tp'), may hold values from -0.125 to 0.125
Outputs:
- mixed: bfloat16 [16384, 2048], P('ep', 'tp')
Inputs may be any that keep to these rules, and one draw needn't show every extreme that they name: `expert_ids`: each row names 4 different experts. In the rows of one device no expert is named by more than 32 rows, and in every draw some expert is named by exactly 32 rows of some device. `gate_weight`: independent entries of mean zero, drawn for each expert separately. `up_weight`: independent entries of mean zero, drawn for each expert separately.
All inputs are finite; a program needn't handle non-finite values.
Results may differ from a plain program's by a relative error of at most 0.014.
Values may be sent and summed in bfloat16 or wider, within the bound.
A program may use at most 128 MiB of HBM per device.

v0:
```python
import jax
import jax.numpy as jnp
from jax import lax
from jax.sharding import PartitionSpec as P


def grouped_exchange(x, axis, split_dim, concat_dim, work, item_dim, out_dim):
    items = jax.tree.leaves(x)[0].shape[item_dim]
    count = 2 if items % 2 == 0 else 1
    gathered = []
    for k in range(count):
        group = jax.tree.map(
            lambda a: lax.slice_in_dim(
                a, k * (items // count), (k + 1) * (items // count), axis=item_dim
            ),
            x,
        )
        gathered.append(
            work(
                lax.all_to_all(
                    group, axis, split_axis=split_dim, concat_axis=concat_dim, tiled=True
                )
            )
        )
    return jax.tree.map(lambda *parts: jnp.concatenate(parts, axis=out_dim), *gathered)


def per_device(tokens, norm_gain, expert_ids, route_weights, gate_weight, up_weight, down_weight):
    tok_dev, width = tokens.shape
    top = expert_ids.shape[1]
    n_ep = lax.axis_size("ep")
    n_tp = lax.axis_size("tp")
    exp_dev = gate_weight.shape[0]
    experts = exp_dev * n_ep
    capacity = 2 * tok_dev * top // experts
    quarter = width // n_tp
    values = tokens.astype(jnp.float32)
    scale = lax.rsqrt(jnp.mean(values * values, axis=1, keepdims=True) + 1e-06)
    normed = (values * scale * norm_gain[None, :]).astype(jnp.bfloat16)
    flat = expert_ids.reshape(-1)
    count = flat.shape[0]
    onehot = (flat[:, None] == jnp.arange(experts, dtype=jnp.int32)[None, :]).astype(jnp.int32)
    before = jnp.cumsum(onehot, axis=0) - onehot
    slot = jnp.sum(before * onehot, axis=1)
    position = flat * capacity + slot
    source_tok = jnp.arange(count, dtype=jnp.int32) // top
    buffer_tok = jnp.zeros((experts * capacity,), jnp.int32).at[position].set(source_tok)
    buffer_live = jnp.zeros((experts * capacity,), jnp.int32).at[position].set(1)

    def finish(received):
        gate = jnp.einsum(
            "sxcd,xdf->sxcf", received, gate_weight, preferred_element_type=jnp.float32
        )
        upper = jnp.einsum(
            "sxcd,xdf->sxcf", received, up_weight, preferred_element_type=jnp.float32
        )
        gate = jnp.minimum(gate, 7.0)
        upper = jnp.clip(upper, -7.0, 7.0)
        hidden = ((upper + 1.0) * (gate * jax.nn.sigmoid(1.702 * gate))).astype(jnp.bfloat16)
        partial_value = jnp.einsum(
            "sxcf,xfd->sxcd", hidden, down_weight, preferred_element_type=jnp.float32
        )
        rounded = partial_value.astype(jnp.bfloat16)
        summed = (
            lax.psum_scatter(rounded, "tp", scatter_dimension=3, tiled=True)
            .astype(jnp.float32)
            .astype(jnp.bfloat16)
        )
        return lax.all_to_all(summed, "ep", split_axis=0, concat_axis=0, tiled=True)

    columns = lax.dynamic_slice_in_dim(normed, lax.axis_index("tp") * quarter, quarter, 1)
    outgoing = jnp.where(buffer_live[:, None] > 0, columns[buffer_tok], jnp.zeros((), jnp.bfloat16))
    outgoing = outgoing.reshape(n_ep, exp_dev, capacity, quarter)

    def widen_finish(received):
        return finish(lax.all_gather(received, "tp", axis=3, tiled=True))

    returned = grouped_exchange(outgoing, "ep", 0, 0, widen_finish, 2, 2)
    returned = returned.reshape(experts * capacity, quarter)
    picked = returned[position].reshape(tok_dev, top, quarter)
    mixed = jnp.sum(route_weights[:, :, None] * picked.astype(jnp.float32), axis=1)
    return mixed.astype(jnp.bfloat16)


def solution(mesh):
    in_specs = (
        P("ep", None),
        P(),
        P("ep", None),
        P("ep", None),
        P("ep", None, "tp"),
        P("ep", None, "tp"),
        P("ep", "tp", None),
    )
    out_specs = P("ep", "tp")
    return jax.shard_map(
        per_device, mesh=mesh, in_specs=in_specs, out_specs=out_specs, check_vma=False
    )
```

profile of v0, /device:TPU:1, one launch (start us, length us, event | category | flops | bytes accessed | tf_op | source)
XLA Modules:
  0.0 356.5 jit_solution(11833789574535953391)
XLA Ops:
  6.5 0.0 copy-start
  6.5 0.0 copy-start.1
  6.5 0.0 all-gather.3.cloned.1.call-start
  6.5 0.0 copy-start.2
  6.5 3.0 convert_element_type.58
  9.5 0.0 copy-done.1
  9.5 0.3 multiply_reduce_fusion.1
  9.8 0.0 copy-done.2
  9.8 0.1 copy.17
  10.0 0.1 eq.29
  10.1 0.1 eq.25
  10.3 18.0 %reduce-window.6 = s32[64,8,128]{2,1,0:T(8,128)S(1)} reduce-window(s32[64,8,128]{2,1,0:T(8,128)S(1)} %fusion.65, s32[]{:T(128)} %constant.19.clone.1), window={size=1x1x128 pad=0_0x0_0x127_0}, to_apply=%region_0.0 | reduce-window | flops 8323072 | bytes 524292 | tf_op jit(solution)/shard_map/reduce-window
  28.3 0.1 slice.20
  28.4 0.1 copy.19
  28.6 0.1 copy.20
  28.7 0.1 broadcast_add_fusion
  28.8 0.1 copy.16
  29.0 0.1 mul.70
  29.1 0.1 fusion.64
  29.2 4.3 %scatter_custom_fusion.1 = s32[2048]{0:T(1024)S(1)} fusion(s32[1024]{0:T(1024)S(1)} %bitcast.179, s32[1024]{0:T(1024)S(1)} %add_select_fusion, s32[]{:T(128)} %constant.19.clone.1), kind=kCustom, calls=%fused_computation.72 | custom fusion | bytes 8196 | tf_op jit(solution)/shard_map/scatter | solution.py:47
  33.5 4.3 %scatter_custom_fusion = s32[2048]{0:T(1024)S(1)} fusion(s32[1024]{0:T(1024)S(1)} %bitcast.180, s32[1024]{0:T(1024)S(1)} %broadcast.149, s32[]{:T(128)} %constant.19.clone.1), kind=kCustom, calls=%fused_computation.75 | custom fusion | bytes 8196 | tf_op jit(solution)/shard_map/scatter | solution.py:48
  37.9 0.1 broadcast_in_dim.29
  38.0 0.8 dynamic-slice
  38.7 1.1 fusion.61
  39.9 9.2 %gather_fusion = bf16[2048,512]{1,0:T(8,128)(2,1)} fusion(bf16[256,512]{1,0:T(8,128)(2,1)S(1)} %fusion.61, s32[2048]{0:T(1024)S(1)} %fusion.66), kind=kCustom, calls=%fused_computation | custom fusion | bytes 4202496 | tf_op jit(solution)/shard_map/gather | solution.py:72
  49.0 1.8 broadcast_select_fusion
  50.8 0.2 fusion.82
  51.0 41.0 %all_to_all.20 = bf16[64,1,16,512]{3,2,1,0:T(8,128)(2,1)} all-to-all(bf16[64,1,16,512]{3,2,1,0:T(8,128)(2,1)S(1)} %get-tuple-element.5), channel_id=1, replica_groups=mesh['ep'=64,'tp'=4] {'ep'}, dimensions={0} | all-to-all | bytes 2097152 | tf_op jit(solution)/shard_map/all_to_all | solution.py:20
  92.0 0.0 all-gather.3.cloned.1.call-update
  92.1 0.0 all-gather.5.cloned.1.call-start
  92.1 34.3 %all_to_all.21 = bf16[64,1,16,512]{3,2,1,0:T(8,128)(2,1)} all-to-all(bf16[64,1,16,512]{3,2,1,0:T(8,128)(2,1)S(1)} %get-tuple-element.6), channel_id=1, replica_groups=mesh['ep'=64,'tp'=4] {'ep'}, dimensions={0} | all-to-all | bytes 2097152 | tf_op jit(solution)/shard_map/all_to_all | solution.py:20
  126.5 0.0 all-gather.5.cloned.1.call-update
  126.5 0.0 reduce-scatter.3.cloned.1.call-start
  126.5 13.4 %all-gather.3.cloned.1.call-done = bf16[64,1,16,2048]{3,2,0,1:T(8,128)(2,1)} async-done(((bf16[64,1,16,512]{3,2,0,1:T(8,128)(2,1)}), bf16[64,1,16,2048]{3,2,0,1:T(8,128)(2,1)}) %all-gather.3.cloned.1.call-update) | async-done | bytes 4194320 | tf_op jit(solution)/shard_map/all_gather | solution.py:76
  139.9 6.5 %fusion.6 = f32[64,16,512]{2,1,0:T(8,128)} fusion(bf16[64,1,16,2048]{3,2,0,1:T(8,128)(2,1)} %all-gather.3.cloned.1.call-done, bf16[1,2048,512]{2,1,0:T(8,128)(2,1)} %param.12), kind=kOutput, calls=%fused_computation.10 | convolution fusion | flops 2147483648 | bytes 8388608 | tf_op jit(solution)/shard_map/sxcd,xdf->sxcf/dot_general | solution.py:54
  146.5 0.0 copy-done
  146.5 10.3 %convert_bitcast_fusion.1 = bf16[64,1,16,2048]{3,2,0,1:T(8,128)(2,1)} fusion(bf16[1,512,2048]{2,1,0:T(8,128)(2,1)S(1)} %copy-done, bf16[1,2048,512]{2,1,0:T(8,128)(2,1)} %param.11, bf16[64,1,16,2048]{3,2,0,1:T(8,128)(2,1)} %all-gather.3.cloned.1.call-done, f32[64,16,512]{2,1,0:T(8,128)} %fusion.6), kind=kOutput, calls=%fused_computation.13 | convolution fusion | flops 4302307328 | bytes 14680064 | tf_op jit(solution)/shard_map/sxcf,xfd->sxcd/dot_general | solution.py:60
  156.8 0.0 reduce-scatter.3.cloned.1.call-update
  156.8 0.2 reduce-scatter.5.cloned.1.call-start
  157.0 35.8 %all-gather.5.cloned.1.call-done = bf16[64,1,16,2048]{3,2,0,1:T(8,128)(2,1)} async-done(((bf16[64,1,16,512]{3,2,0,1:T(8,128)(2,1)}), bf16[64,1,16,2048]{3,2,0,1:T(8,128)(2,1)}) %all-gather.5.cloned.1.call-update) | async-done | bytes 4194320 | tf_op jit(solution)/shard_map/all_gather | solution.py:76
  192.9 6.6 %fusion.2 = f32[64,16,512]{2,1,0:T(8,128)} fusion(bf16[64,1,16,2048]{3,2,0,1:T(8,128)(2,1)} %all-gather.5.cloned.1.call-done, bf16[1,2048,512]{2,1,0:T(8,128)(2,1)} %param.12), kind=kOutput, calls=%fused_computation.6 | convolution fusion | flops 2147483648 | bytes 8388608 | tf_op jit(solution)/shard_map/sxcd,xdf->sxcf/dot_general | solution.py:54
  199.5 10.3 %convert_bitcast_fusion = bf16[64,1,16,2048]{3,2,0,1:T(8,128)(2,1)} fusion(bf16[1,512,2048]{2,1,0:T(8,128)(2,1)S(1)} %copy-done, bf16[1,2048,512]{2,1,0:T(8,128)(2,1)} %param.11, bf16[64,1,16,2048]{3,2,0,1:T(8,128)(2,1)} %all-gather.5.cloned.1.call-done, f32[64,16,512]{2,1,0:T(8,128)} %fusion.2), kind=kOutput, calls=%fused_computation.12 | convolution fusion | flops 4302307328 | bytes 14680064 | tf_op jit(solution)/shard_map/sxcf,xfd->sxcd/dot_general | solution.py:60
  209.8 0.0 reduce-scatter.5.cloned.1.call-update
  209.8 35.5 %reduce-scatter.3.cloned.1.call-done = bf16[64,1,16,512]{3,2,0,1:T(8,128)(2,1)} async-done(((bf16[64,1,16,2048]{3,2,0,1:T(8,128)(2,1)}), bf16[64,1,16,512]{3,2,0,1:T(8,128)(2,1)}) %reduce-scatter.3.cloned.1.call-update) | async-done | bytes 1048592 | tf_op jit(solution)/shard_map/reduce_scatter | solution.py:65
  245.3 0.0 copy-start.3
  245.3 10.8 %all-to-all-start.1 = ((bf16[64,1,16,512]{3,2,1,0:T(8,128)(2,1)}), bf16[64,1,16,512]{3,2,1,0:T(8,128)(2,1)S(1)}, u32[]{:S(2)}, u32[]{:S(2)}) async-start(bf16[64,1,16,512]{3,2,1,0:T(8,128)(2,1)} %bitcast.174), calls=%async_computation.2 | async-start | bytes 2097152 | tf_op jit(solution)/shard_map/all_to_all | solution.py:69
  256.2 40.7 %reduce-scatter.5.cloned.1.call-done = bf16[64,1,16,512]{3,2,0,1:T(8,128)(2,1)} async-done(((bf16[64,1,16,2048]{3,2,0,1:T(8,128)(2,1)}), bf16[64,1,16,512]{3,2,0,1:T(8,128)(2,1)}) %reduce-scatter.5.cloned.1.call-update) | async-done | bytes 1048592 | tf_op jit(solution)/shard_map/reduce_scatter | solution.py:65
  296.9 0.0 all-to-all-done.1
  296.9 10.9 %all-to-all-start.3 = ((bf16[64,1,16,512]{3,2,1,0:T(8,128)(2,1)}), bf16[64,1,16,512]{3,2,1,0:T(8,128)(2,1)}, u32[]{:S(2)}, u32[]{:S(2)}) async-start(bf16[64,1,16,512]{3,2,1,0:T(8,128)(2,1)} %bitcast.175), calls=%async_computation.5 | async-start | bytes 2097152 | tf_op jit(solution)/shard_map/all_to_all | solution.py:69
  307.9 0.0 copy-done.3
  307.9 0.1 copy.15
  308.0 27.9 %all-to-all-done.3 = bf16[64,1,16,512]{3,2,1,0:T(8,128)(2,1)} async-done(((bf16[64,1,16,512]{3,2,1,0:T(8,128)(2,1)}), bf16[64,1,16,512]{3,2,1,0:T(8,128)(2,1)}, u32[]{:S(2)}, u32[]{:S(2)}) %all-to-all-start.3) | async-done | bytes 1048608 | tf_op jit(solution)/shard_map/all_to_all | solution.py:69
  335.9 2.8 pad_maximum_fusion
  338.7 5.8 %gather_fusion.1 = bf16[1024,512]{1,0:T(8,128)(2,1)S(1)} fusion(bf16[2048,512]{1,0:T(8,128)(2,1)} %bitcast.170, s32[1024]{0:T(1024)S(1)} %broadcast_clamp_fusion), kind=kCustom, calls=%fused_computation.1 | custom fusion | bytes 2101248 | tf_op jit(solution)/shard_map/gather | solution.py:80
  344.6 1.7 reshape.139
  346.3 3.7 %multiply_reduce_fusion = bf16[256,512]{1,0:T(8,128)(2,1)} fusion(f32[256,4,512]{2,1,0:T(4,128)} %reshape.139, f32[256,4]{1,0:T(8,128)S(1)} %copy.15), kind=kLoop, calls=%fused_computation.37 | loop fusion | flops 917504 | bytes 2363392 | tf_op jit(solution)/shard_map/reduce_sum | solution.py:81
  (11 shorter events, 0.1 us)
Async XLA Ops:
  6.5 139.9 %copy-start = (bf16[1,512,2048]{2,1,0:T(8,128)(2,1)S(1)}, bf16[1,512,2048]{2,1,0:T(8,128)(2,1)}, u32[]{:S(2)}) copy-start(bf16[1,512,2048]{2,1,0:T(8,128)(2,1)} %param.13) | copy-start | bytes 6291460
  6.5 3.0 copy-start.1
  6.5 133.4 %all-gather.3.cloned.1.call-start = ((), (), s32[]{:S(2)}) async-start(), calls=%async_computation.6 | async-start | bytes 5242880 | tf_op jit(solution)/shard_map/all_gather | solution.py:76
  6.5 3.3 copy-start.2
  92.1 100.8 %all-gather.5.cloned.1.call-start = ((), (), s32[]{:S(2)}) async-start(), calls=%async_computation.8 | async-start | bytes 5242880 | tf_op jit(solution)/shard_map/all_gather | solution.py:76
  126.5 118.8 %reduce-scatter.3.cloned.1.call-start = ((), (), s32[]{:S(2)}) async-start(), calls=%async_computation.7 | async-start | bytes 5242880 | tf_op jit(solution)/shard_map/reduce_scatter | solution.py:65
  156.8 140.1 %reduce-scatter.5.cloned.1.call-start = ((), (), s32[]{:S(2)}) async-start(), calls=%async_computation.9 | async-start | bytes 5242880 | tf_op jit(solution)/shard_map/reduce_scatter | solution.py:65
  245.3 62.5 %copy-start.3 = (f32[256,4]{0,1:T(4,128)S(1)}, f32[256,4]{0,1:T(4,128)}, u32[]{:S(2)}) copy-start(f32[256,4]{0,1:T(4,128)} %param.10) | copy-start | bytes 12292
  245.3 51.6 %all-to-all-start.1 = ((bf16[64,1,16,512]{3,2,1,0:T(8,128)(2,1)}), bf16[64,1,16,512]{3,2,1,0:T(8,128)(2,1)S(1)}, u32[]{:S(2)}, u32[]{:S(2)}) async-start(bf16[64,1,16,512]{3,2,1,0:T(8,128)(2,1)} %bitcast.174), calls=%async_computation.2 | async-start | bytes 2097152 | tf_op jit(solution)/shard_map/all_to_all | solution.py:69
  296.9 39.0 %all-to-all-start.3 = ((bf16[64,1,16,512]{3,2,1,0:T(8,128)(2,1)}), bf16[64,1,16,512]{3,2,1,0:T(8,128)(2,1)}, u32[]{:S(2)}, u32[]{:S(2)}) async-start(bf16[64,1,16,512]{3,2,1,0:T(8,128)(2,1)} %bitcast.175), calls=%async_computation.5 | async-start | bytes 2097152 | tf_op jit(solution)/shard_map/all_to_all | solution.py:69
Sparse Core Ops, SparseCore 0:
  92.2 47.6 all-gather.2
  141.7 51.1 all-gather.4
  195.4 49.8 reduce-scatter.2
  247.7 49.1 reduce-scatter.4
where the time goes:
time: 357 us
  waiting for transfers between devices  154 us (43%)
  blocking collectives  75.4 us (21%)
  matrix products  33.7 us (9%)
  other arithmetic  30.9 us (9%)
  local copies, waits for them, and re-layouts  27.5 us (8%)
  starting transfers between devices  22.1 us (6%)
  between operations  13.4 us (4%)
    reduce_scatter x2, waiting for transfers between devices, finish(): lax.psum_scatter(rounded, 'tp', scatter_dimension=3, tiled=True)  76.3 us
    all_to_all x2, blocking collectives, grouped_exchange(): lax.all_to_all(group, axis, split_axis=split_dim, concat_axis=concat_dim,...  75.4 us
    all_gather x2, waiting for transfers between devices, widen_finish(): return finish(lax.all_gather(received, 'tp', axis=3, tiled=True))  49.2 us
    all_to_all x2, waiting for transfers between devices, finish(): return lax.all_to_all(summed, 'ep', split_axis=0, concat_axis=0, tiled=True)  27.9 us
    all_to_all x2, starting transfers between devices, finish(): return lax.all_to_all(summed, 'ep', split_axis=0, concat_axis=0, tiled=True)  21.7 us
    dot_general x2, matrix products, finish(): jnp.einsum('sxcf,xfd->sxcd', hidden, down_weight, preferred_element_type=...  20.6 us
    another operation x3, other arithmetic  18.2 us
    dot_general x2, matrix products, finish(): jnp.einsum('sxcd,xdf->sxcf', received, up_weight, preferred_element_type=...  13.1 us
  transfers between devices with their start and end apart: 6, of which 5 were waited for; matrix products, arithmetic and copies ran while one was open for 10% of the time, Pallas kernels for 0%

commit v1 on v0

v1 whole, which is shorter than its diff:
```python
import jax
import jax.numpy as jnp
from jax import lax
from jax.experimental import pallas as pl
from jax.experimental.pallas import tpu as pltpu
from jax.sharding import PartitionSpec as P

MESH = pl.DeviceIdType.MESH
NZ = 8
NJ = 8
NY = 4
TOK = 256
CAP = 32
W = 2048
Q = 512
ROWS = NJ * CAP
META = 16
R, L = 0, 1
A, B = 0, 1
HALF = NZ // 2
PARTS = 2
BF = jnp.bfloat16
F32 = jnp.float32


def top_hop(direction, chunk):
    return HALF if direction == chunk else HALF - 1


SCHEDULE = (
    "D00", "D01", "Y00", "Z1100", "Z0100", "Z1101", "D10", "Z0101", "Z1110", "D70", "Y10", "Z1111",
    "Z0200", "D11", "Y70", "Z1200", "Z1201", "D20", "Z0201", "Z1210", "Z0300", "D60", "Y20", "Z1211",
    "Z0301", "D50", "Y60", "Z0111", "Z0110", "D21", "Z0400", "Z0401", "Y50", "D40", "Z0211", "Z1300",
    "D71", "Z1311", "Z0210", "Z1301", "Z1310", "Y40", "D30", "Z0311", "D61", "Z1411", "Z1410", "D41",
    "Y30", "Z0310", "D51", "D31", "F40", "F50", "F30", "G40", "F60", "G50", "F20", "C4", "G30", "r0401",
    "r1410", "r0400", "F70", "r1411", "C5", "r1301", "r1310", "C3", "r0310", "G60", "r0300", "r1300",
    "G20", "r1311", "r0311", "F10", "C6", "r0301", "r1201", "G70", "C2", "r0200", "F00", "r1211",
    "r1200", "r0211", "r0210", "G10", "C7", "r0201", "r1210", "r1111", "G00", "C1", "r0111", "r1110",
    "r1101", "r0110", "r0101", "r1100", "r0100", "C0", "E1", "E0", "O1", "O0",
)


def kernel(
    tok_ref, gain_ref, ids_ref, rw_ref, wg_ref, wu_ref, wd_ref, out_ref,
    za, zb, xs, xf, wgu, wdn, hid, ps, yr, xs2, cr, tsum, rin, rout, exs, exr, info_ref,
    w_sem, z_s, z_r, x_s, x_r, y_s, y_r, p_s, p_r, q_s, q_r, c_s, c_r, e_s, e_r,
):
    me = lax.axis_index("ep")
    y = lax.axis_index("tp")
    z = me // NJ
    j = lax.rem(me, NJ)
    up_z = lax.rem(z + 1, NZ) * NJ + j
    down_z = lax.rem(z + NZ - 1, NZ) * NJ + j
    y_up = lax.rem(y + 1, NY)
    y_far = lax.rem(y + 2, NY)
    y_down = lax.rem(y + 3, NY)
    zdev = ((up_z, y), (down_z, y))
    ydev = ((me, y_up), (me, y_down))

    def peer(o):
        return lax.rem(j + o, NJ)

    def quarter(i):
        return pl.ds(pl.multiple_of((y, y_far, y_down, y_up)[i] * Q, Q), Q)

    weights = []
    for i in range(4):
        weights.append((wg_ref.at[0, quarter(i), :], wgu.at[pl.ds(i * Q, Q), pl.ds(0, Q)]))
        weights.append((wu_ref.at[0, quarter(i), :], wgu.at[pl.ds(i * Q, Q), pl.ds(Q, Q)]))
        weights.append((wd_ref.at[0, :, quarter(i)], wdn.at[:, pl.ds(i * Q, Q)]))
    weights = [pltpu.make_async_copy(s, d, w_sem.at[i]) for i, (s, d) in enumerate(weights)]
    for copy in weights:
        copy.start()

    barrier = pltpu.get_barrier_semaphore()
    partners = list(zdev) + list(ydev) + [(me, y_far)]
    partners += [(z * NJ + peer(o), y) for o in range(1, NJ)]
    for device in partners:
        pl.semaphore_signal(barrier, inc=1, device_id=device, device_id_type=MESH)

    sends = []

    def send(src, dst, ssem, rsem, device):
        copy = pltpu.make_async_remote_copy(
            src_ref=src, dst_ref=dst, send_sem=ssem, recv_sem=rsem,
            device_id=device, device_id_type=MESH,
        )
        copy.start()
        return copy

    def await_bytes(ref, sem):
        pltpu.make_async_copy(ref, ref, sem).wait()

    ids = ids_ref[...].astype(F32)
    expert = lax.broadcasted_iota(jnp.int32, (NZ * NJ, TOK), 0).astype(F32)
    hits = [ids[k : k + 1, :] == expert for k in range(4)]
    named = jnp.where(hits[0] | hits[1] | hits[2] | hits[3], 1.0, 0.0).astype(BF)
    earlier = lax.broadcasted_iota(jnp.int32, (TOK, TOK), 0) < lax.broadcasted_iota(
        jnp.int32, (TOK, TOK), 1
    )
    before = jnp.dot(named, jnp.where(earlier, 1.0, 0.0).astype(BF), preferred_element_type=F32)
    info_ref[...] = jnp.zeros_like(info_ref)
    info_ref[pl.ds(0, 4), :] = ids
    for k in range(4):
        slot = jnp.sum(jnp.where(hits[k], before, 0.0), axis=0, keepdims=True)
        info_ref[pl.ds(4 + k, 1), :] = slot
    info_ref[pl.ds(8, 4), :] = rw_ref[...]
    za[0, pl.ds(TOK, META), pl.ds(0, TOK)] = info_ref[...].astype(BF)
    za[0, pl.ds(TOK, META), pl.ds(TOK, TOK)] = jnp.zeros((META, TOK), BF)

    values = tok_ref[...].astype(F32)
    scale = lax.rsqrt(jnp.mean(values * values, axis=1, keepdims=True) + 1e-06)
    for i, buf in enumerate((za, zb)):
        part = tok_ref[:, quarter(i)].astype(F32) * scale * gain_ref[:, quarter(i)]
        buf[0, pl.ds(0, TOK), :] = part.astype(BF)

    pl.semaphore_wait(barrier, len(partners))

    def piece(chunk, part):
        size = (TOK + META, TOK)[chunk]
        cut = (TOK // 2 + META, TOK // 2)[chunk]
        return pl.ds(0, cut) if part == 0 else pl.ds(cut, size - cut)

    def z_send(direction, hop, chunk, part):
        buf = (za, zb)[chunk]
        here = (-hop if direction == R else hop) % NZ
        there = (-(hop + 1) if direction == R else hop + 1) % NZ
        rows = piece(chunk, part)
        sends.append(
            send(
                buf.at[here, rows], buf.at[there, rows],
                z_s.at[direction, hop, chunk, part], z_r.at[direction, hop, chunk, part],
                zdev[direction],
            )
        )

    def z_step(direction, hop, chunk, part):
        buf = (za, zb)[chunk]
        slot = (-hop if direction == R else hop) % NZ
        await_bytes(buf.at[slot, piece(chunk, part)], z_r.at[direction, hop - 1, chunk, part])
        if hop < top_hop(direction, chunk):
            z_send(direction, hop, chunk, part)

    for chunk in (A, B):
        for part in range(PARTS):
            for direction in (R, L):
                z_send(direction, 0, chunk, part)

    base = (z * ROWS).astype(F32)

    def places(b):
        info = za[b, pl.ds(TOK, META), pl.ds(0, TOK)].astype(F32)
        at = lax.broadcasted_iota(jnp.int32, (ROWS, TOK), 0).astype(F32) + base
        return info, [info[k : k + 1] * CAP + info[4 + k : 5 + k] == at for k in range(4)]

    def rows_of(p):
        return pl.ds(pl.multiple_of(p * CAP, CAP), CAP)

    def exchange(src, dst, ssem, rsem):
        for o in range(1, NJ):
            p = peer(o)
            send(src.at[rows_of(p), :], dst.at[rows_of(j), :], ssem, rsem, (z * NJ + p, y))
        dst[rows_of(j), :] = src[rows_of(j), :]

    def await_exchange(dst, rsem):
        await_bytes(dst.at[pl.ds(0, ROWS - CAP), :], rsem)

    def cols(i):
        return pl.ds(i * Q, Q)

    def dispatch(b, chunk):
        info, at = places(b)
        pick = jnp.where(at[0] | at[1] | at[2] | at[3], 1.0, 0.0).astype(BF)
        block = (za, zb)[chunk][b, pl.ds(0, TOK), :]
        xs[b, chunk] = jnp.dot(pick, block, preferred_element_type=F32).astype(BF)
        exchange(xs.at[b, chunk], xf.at[b, :, cols(chunk)], x_s.at[b, chunk], x_r.at[b, chunk])

    def spread(b):
        await_exchange(xf.at[b, :, cols(A)], x_r.at[b, A])
        for side in range(2):
            sends.append(
                send(
                    xf.at[b, :, cols(A)], xf.at[b, :, cols(2 + side)],
                    y_s.at[side, b], y_r.at[side, b], ydev[side],
                )
            )

    def experts(b):
        await_exchange(xf.at[b, :, cols(B)], x_r.at[b, B])
        for side in range(2):
            await_bytes(xf.at[b, :, cols(2 + side)], y_r.at[side, b])
        rows = xf[b]
        for n in range(2):
            gate = jnp.dot(rows, wgu[:, pl.ds(n * 256, 256)], preferred_element_type=F32)
            upper = jnp.dot(rows, wgu[:, pl.ds(Q + n * 256, 256)], preferred_element_type=F32)
            gate = jnp.minimum(gate, 7.0)
            upper = jnp.clip(upper, -7.0, 7.0)
            hid[:, pl.ds(n * 256, 256)] = (
                (upper + 1.0) * (gate * jax.nn.sigmoid(1.702 * gate))
            ).astype(BF)
        for i in (2, 3, 1, 0):
            part = jnp.dot(hid[...], wdn[:, cols(i)], preferred_element_type=F32)
            ps[b, i] = part.astype(BF)
            if i >= 2:
                side = 3 - i
                sends.append(
                    send(
                        ps.at[b, i], yr.at[side, b],
                        p_s.at[side, b], p_r.at[side, b], ydev[side],
                    )
                )
            elif i == 1:
                exchange(ps.at[b, 1], cr.at[b, B], q_s.at[b, B], q_r.at[b, B])

    def give_back(b):
        for side in range(2):
            await_bytes(yr.at[side, b], p_r.at[side, b])
        total = ps[b, 0].astype(F32) + yr[0, b].astype(F32) + yr[1, b].astype(F32)
        xs2[b] = total.astype(BF)
        exchange(xs2.at[b], cr.at[b, A], q_s.at[b, A], q_r.at[b, A])

    def combine(b):
        for chunk in (A, B):
            await_exchange(cr.at[b, chunk], q_r.at[b, chunk])
        info, at = places(b)
        weight = jnp.zeros((ROWS, TOK), F32)
        for k in range(4):
            weight = jnp.where(at[k], info[8 + k : 9 + k], weight)
        weight = weight.astype(BF)
        for chunk in (A, B):
            tsum[b, chunk] = lax.dot_general(
                weight, cr[b, chunk], (((0,), (0,)), ((), ())), preferred_element_type=F32
            )

    def span(part):
        return pl.ds(part * (TOK // PARTS), TOK // PARTS)

    def reduce_step(direction, hop, chunk, part):
        b = (hop if direction == R else -hop) % NZ
        value = tsum[b, chunk, span(part), :]
        if hop < top_hop(direction, chunk):
            came = rin.at[direction, hop, chunk, span(part), :]
            await_bytes(came, c_r.at[direction, hop, chunk, part])
            value = value + came[...].astype(F32)
        src = rout.at[direction, hop - 1, chunk, span(part), :]
        src[...] = value.astype(BF)
        sends.append(
            send(
                src, rin.at[direction, hop - 1, chunk, span(part), :],
                c_s.at[direction, hop - 1, chunk, part], c_r.at[direction, hop - 1, chunk, part],
                zdev[direction],
            )
        )

    def arrived(chunk, part):
        total = tsum[0, chunk, span(part), :]
        for direction in (R, L):
            came = rin.at[direction, 0, chunk, span(part), :]
            await_bytes(came, c_r.at[direction, 0, chunk, part])
            total = total + came[...].astype(F32)
        return total

    def finish_far(part):
        exs[span(part), :] = arrived(B, part).astype(BF)
        sends.append(
            send(
                exs.at[span(part), :], exr.at[span(part), :],
                e_s.at[part], e_r.at[part], (me, y_far),
            )
        )

    def finish_own(part):
        own = arrived(A, part)
        await_bytes(exr.at[span(part), :], e_r.at[part])
        out_ref[span(part), :] = (own + exr[span(part), :].astype(F32)).astype(BF)

    waiting = list(weights)
    for name in SCHEDULE:
        arg = [int(d) for d in name[1:]]
        if name[0] == "F":
            while waiting:
                waiting.pop().wait()
        if name[0] in "YFG":
            arg = arg[:1]
        {
            "Z": z_step, "D": dispatch, "Y": spread, "F": experts, "G": give_back,
            "C": combine, "r": reduce_step, "E": finish_far, "O": finish_own,
        }[name[0]](*arg)

    for copy in sends:
        copy.wait_send()
    for b in range(NZ):
        for chunk in (A, B):
            await_exchange(xs.at[b, chunk], x_s.at[b, chunk])
        await_exchange(xs2.at[b], q_s.at[b, A])
        await_exchange(ps.at[b, 1], q_s.at[b, B])


def per_device(tokens, norm_gain, expert_ids, route_weights, gate_weight, up_weight, down_weight):
    vmem = pl.BlockSpec(memory_space=pltpu.VMEM)
    hbm = pl.BlockSpec(memory_space=pl.ANY)
    dma = pltpu.SemaphoreType.DMA
    return pl.pallas_call(
        kernel,
        out_shape=jax.ShapeDtypeStruct((TOK, Q), BF),
        in_specs=[vmem, vmem, vmem, vmem, hbm, hbm, hbm],
        out_specs=vmem,
        scratch_shapes=[
            pltpu.VMEM((NZ, TOK + META, Q), BF),
            pltpu.VMEM((NZ, TOK, Q), BF),
            pltpu.VMEM((NZ, 2, ROWS, Q), BF),
            pltpu.VMEM((NZ, ROWS, W), BF),
            pltpu.VMEM((W, 2 * Q), BF),
            pltpu.VMEM((Q, W), BF),
            pltpu.VMEM((ROWS, Q), BF),
            pltpu.VMEM((NZ, 4, ROWS, Q), BF),
            pltpu.VMEM((2, NZ, ROWS, Q), BF),
            pltpu.VMEM((NZ, ROWS, Q), BF),
            pltpu.VMEM((NZ, 2, ROWS, Q), BF),
            pltpu.VMEM((NZ, 2, TOK, Q), F32),
            pltpu.VMEM((2, HALF, 2, TOK, Q), BF),
            pltpu.VMEM((2, HALF, 2, TOK, Q), BF),
            pltpu.VMEM((TOK, Q), BF),
            pltpu.VMEM((TOK, Q), BF),
            pltpu.VMEM((META, TOK), F32),
            dma((12,)),
            dma((2, HALF, 2, PARTS)), dma((2, HALF, 2, PARTS)),
            dma((NZ, 2)), dma((NZ, 2)),
            dma((2, NZ)), dma((2, NZ)),
            dma((2, NZ)), dma((2, NZ)),
            dma((NZ, 2)), dma((NZ, 2)),
            dma((2, HALF, 2, PARTS)), dma((2, HALF, 2, PARTS)),
            dma((PARTS,)), dma((PARTS,)),
        ],
        compiler_params=pltpu.CompilerParams(
            collective_id=0, has_side_effects=True, vmem_limit_bytes=67_000_000
        ),
        name="moe",
    )(
        tokens, norm_gain.reshape(1, W), expert_ids.T, route_weights.T,
        gate_weight, up_weight, down_weight,
    )


def solution(mesh):
    in_specs = (
        P("ep", None),
        P(),
        P("ep", None),
        P("ep", None),
        P("ep", None, "tp"),
        P("ep", None, "tp"),
        P("ep", "tp", None),
    )
    out_specs = P("ep", "tp")
    return jax.shard_map(
        per_device, mesh=mesh, in_specs=in_specs, out_specs=out_specs, check_vma=False
    )
```

time: 357 us -> 132 us (0.37)
  waiting for transfers between devices: 154 us -> 0 us
  Pallas kernels: 0 us -> 130 us
  blocking collectives: 75.4 us -> 0 us
  matrix products: 33.7 us -> 0 us
  other arithmetic: 30.9 us -> 0 us
  local copies, waits for them, and re-layouts: 27.5 us -> 1.67 us
  starting transfers between devices: 22.1 us -> 0 us
  between operations: 13.4 us -> 0.01 us
    pallas_call x0 -> x1, Pallas kernels: none -> 130 us  [per_device(): pl.pallas_call(kernel, out_shape=jax.ShapeDtypeStruct((TOK, Q), BF), in_s...]
    reduce_scatter x2 -> x0, waiting for transfers between devices: 76.3 us -> none  [finish(): lax.psum_scatter(rounded, 'tp', scatter_dimension=3, tiled=True)]
    all_to_all x2 -> x0, blocking collectives: 75.4 us -> none  [grouped_exchange(): lax.all_to_all(group, axis, split_axis=split_dim, concat_axis=concat_dim,...]
    all_gather x2 -> x0, waiting for transfers between devices: 49.2 us -> none  [widen_finish(): return finish(lax.all_gather(received, 'tp', axis=3, tiled=True))]
    dot_general x4 -> x0, matrix products: 33.7 us -> none  [the longest x2 20.6 us: finish(): jnp.einsum('sxcf,xfd->sxcd', hidden, down_weight, preferred_element_type=...]
    all_to_all x2 -> x0, waiting for transfers between devices: 27.9 us -> none  [finish(): return lax.all_to_all(summed, 'ep', split_axis=0, concat_axis=0, tiled=True)]
    all_to_all x2 -> x0, starting transfers between devices: 21.7 us -> none  [finish(): return lax.all_to_all(summed, 'ep', split_axis=0, concat_axis=0, tiled=True)]
    another operation x3 -> x0, other arithmetic: 18.2 us -> none
  transfers between devices with their start and end apart: 6 -> 0, of which waited for: 5 -> 0; matrix products, arithmetic and copies ran while one was open for 10% -> 0% of each run, Pallas kernels for 0% -> 0%
where the time goes in v1:
time: 132 us
  Pallas kernels  130 us (98%)
  local copies, waits for them, and re-layouts  1.67 us (1%)
    pallas_call x1, Pallas kernels, per_device(): pl.pallas_call(kernel, out_shape=jax.ShapeDtypeStruct((TOK, Q), BF), in_s...  130 us

profile of v1, /device:TPU:1, one launch (start us, length us, event | category | flops | bytes accessed | tf_op | source)
XLA Modules:
  0.0 132.1 jit_solution(6149223939395060934)
XLA Ops:
  0.0 130.4 %moe.1 = bf16[256,512]{1,0:T(8,128)(2,1)} custom-call(bf16[256,2048]{1,0:T(8,128)(2,1)} %tok_ref.1, f32[1,2048]{1,0:T(1,128)} %bitcast.3, s32[4,256]{1,0:T(4,128)} %bitcast.4, f32[4,256]{1,0:T(4,128)} %bitcast.5, bf16[1,2048,512]{2,1,0:T(8,128)(2,1)} %wg_ref.1, bf16[1,2048,512]{2,1,0:T(8,128)(2,1)} %wu_ref.1, bf16[1,512,2048]{2,1,0:T(8,128)(2,1)} %wd_ref.1), custom_call_target="tpu_custom_call" | custom-call | tf_op jit(solution)/shard_map/moe/pallas_call | solution.py:303
  130.4 1.7 %copy.9 = bf16[256,512]{1,0:T(8,128)(2,1)} copy(bf16[256,512]{1,0:T(8,128)(2,1)} %moe.1) | data formatting | bytes 524288

commit v2 on v1

--- a/solution.py
+++ b/solution.py
@@ -19,6 +19,9 @@
 A, B = 0, 1
 HALF = NZ // 2
 PARTS = 2
+CUTS = 1
+SUB = CAP // CUTS
+PIECE = ROWS // CUTS
 BF = jnp.bfloat16
 F32 = jnp.float32
 
@@ -28,22 +31,23 @@
 
 
 SCHEDULE = (
-    "D00", "D01", "Y00", "Z1100", "Z0100", "Z1101", "D10", "Z0101", "Z1110", "D70", "Y10", "Z1111",
-    "Z0200", "D11", "Y70", "Z1200", "Z1201", "D20", "Z0201", "Z1210", "Z0300", "D60", "Y20", "Z1211",
-    "Z0301", "D50", "Y60", "Z0111", "Z0110", "D21", "Z0400", "Z0401", "Y50", "D40", "Z0211", "Z1300",
-    "D71", "Z1311", "Z0210", "Z1301", "Z1310", "Y40", "D30", "Z0311", "D61", "Z1411", "Z1410", "D41",
-    "Y30", "Z0310", "D51", "D31", "F40", "F50", "F30", "G40", "F60", "G50", "F20", "C4", "G30", "r0401",
-    "r1410", "r0400", "F70", "r1411", "C5", "r1301", "r1310", "C3", "r0310", "G60", "r0300", "r1300",
-    "G20", "r1311", "r0311", "F10", "C6", "r0301", "r1201", "G70", "C2", "r0200", "F00", "r1211",
-    "r1200", "r0211", "r0210", "G10", "C7", "r0201", "r1210", "r1111", "G00", "C1", "r0111", "r1110",
-    "r1101", "r0110", "r0101", "r1100", "r0100", "C0", "E1", "E0", "O1", "O0",
+    "D00", "Z1100", "D01", "Z1101", "Z0100", "Z0101", "D70", "Y00", "Z1110", "D10", "Z1111", "Y70",
+    "D11", "Y10", "Z0200", "Z0201", "D60", "Z1201", "Z0300", "Z1200", "Z0110", "D20", "Z1210", "Y60",
+    "Z0301", "D50", "Z0111", "Z1301", "D71", "Y20", "Z1211", "D21", "Z0401", "Z1310", "Z0210", "Z1300",
+    "Z0400", "D40", "Y50", "Z0211", "D30", "Z1311", "D61", "Y40", "Z1410", "Z1411", "Z0310", "Z0311",
+    "D51", "D41", "D31", "Y30", "F50", "F40", "F30", "F20", "F60", "C41", "r1410", "r1411", "C31",
+    "r0311", "G40", "C51", "G50", "r0310", "C21", "F10", "r0211", "r1310", "G30", "C40", "r0210",
+    "r1311", "C61", "r0401", "C50", "r1300", "r0400", "F70", "r1211", "G20", "C11", "r1210", "r1301",
+    "C30", "r0110", "r0301", "G60", "F00", "r0300", "C71", "r1111", "G10", "r0111", "r1110", "C60",
+    "C20", "r0201", "C01", "r0200", "r1201", "G70", "r1200", "C10", "E1", "r0101", "C70", "r1101",
+    "r0100", "E0", "G00", "r1100", "C00", "O1", "O0",
 )
 
 
 def kernel(
-    tok_ref, gain_ref, ids_ref, rw_ref, wg_ref, wu_ref, wd_ref, out_ref,
-    za, zb, xs, xf, wgu, wdn, hid, ps, yr, xs2, cr, tsum, rin, rout, exs, exr, info_ref,
-    w_sem, z_s, z_r, x_s, x_r, y_s, y_r, p_s, p_r, q_s, q_r, c_s, c_r, e_s, e_r,
+    tok_hbm, gain_ref, ids_ref, rw_ref, wg_ref, wu_ref, wd_ref, own_hbm, far_hbm,
+    tok_ref, own_ref, za, zb, xs, xf, wgu, wdn, hid, ps, yr, xs2, cr, tsum, rin, rout, exs, info_ref,
+    t_sem, o_sem, w_sem, z_s, z_r, x_s, x_r, y_s, y_r, p_s, p_r, q_s, q_r, c_s, c_r, e_s, e_r,
 ):
     me = lax.axis_index("ep")
     y = lax.axis_index("tp")
@@ -63,20 +67,21 @@
     def quarter(i):
         return pl.ds(pl.multiple_of((y, y_far, y_down, y_up)[i] * Q, Q), Q)
 
+    tokens = pltpu.make_async_copy(tok_hbm, tok_ref, t_sem)
+    tokens.start()
+
+    barrier = pltpu.get_barrier_semaphore()
+    partners = list(zdev) + list(ydev) + [(me, y_far)]
+    partners += [(z * NJ + peer(o), y) for o in range(1, NJ)]
+    for device in partners:
+        pl.semaphore_signal(barrier, inc=1, device_id=device, device_id_type=MESH)
+
     weights = []
     for i in range(4):
         weights.append((wg_ref.at[0, quarter(i), :], wgu.at[pl.ds(i * Q, Q), pl.ds(0, Q)]))
         weights.append((wu_ref.at[0, quarter(i), :], wgu.at[pl.ds(i * Q, Q), pl.ds(Q, Q)]))
         weights.append((wd_ref.at[0, :, quarter(i)], wdn.at[:, pl.ds(i * Q, Q)]))
     weights = [pltpu.make_async_copy(s, d, w_sem.at[i]) for i, (s, d) in enumerate(weights)]
-    for copy in weights:
-        copy.start()
-
-    barrier = pltpu.get_barrier_semaphore()
-    partners = list(zdev) + list(ydev) + [(me, y_far)]
-    partners += [(z * NJ + peer(o), y) for o in range(1, NJ)]
-    for device in partners:
-        pl.semaphore_signal(barrier, inc=1, device_id=device, device_id_type=MESH)
 
     sends = []
 
@@ -108,6 +113,9 @@
     za[0, pl.ds(TOK, META), pl.ds(0, TOK)] = info_ref[...].astype(BF)
     za[0, pl.ds(TOK, META), pl.ds(TOK, TOK)] = jnp.zeros((META, TOK), BF)
 
+    tokens.wait()
+    for copy in weights:
+        copy.start()
     values = tok_ref[...].astype(F32)
     scale = lax.rsqrt(jnp.mean(values * values, axis=1, keepdims=True) + 1e-06)
     for i, buf in enumerate((za, zb)):
@@ -118,8 +126,9 @@
 
     def piece(chunk, part):
         size = (TOK + META, TOK)[chunk]
-        cut = (TOK // 2 + META, TOK // 2)[chunk]
-        return pl.ds(0, cut) if part == 0 else pl.ds(cut, size - cut)
+        step = TOK // PARTS
+        first = size - TOK
+        return pl.ds(0, step + first) if part == 0 else pl.ds(first + part * step, step)
 
     def z_send(direction, hop, chunk, part):
         buf = (za, zb)[chunk]
@@ -150,11 +159,13 @@
 
     def places(b):
         info = za[b, pl.ds(TOK, META), pl.ds(0, TOK)].astype(F32)
-        at = lax.broadcasted_iota(jnp.int32, (ROWS, TOK), 0).astype(F32) + base
+        row = lax.broadcasted_iota(jnp.int32, (ROWS, TOK), 0)
+        row = lax.rem(row, PIECE) // SUB * CAP + row // PIECE * SUB + lax.rem(row, SUB)
+        at = row.astype(F32) + base
         return info, [info[k : k + 1] * CAP + info[4 + k : 5 + k] == at for k in range(4)]
 
     def rows_of(p):
-        return pl.ds(pl.multiple_of(p * CAP, CAP), CAP)
+        return pl.ds(pl.multiple_of(p * SUB, SUB), SUB)
 
     def exchange(src, dst, ssem, rsem):
         for o in range(1, NJ):
@@ -163,7 +174,10 @@
         dst[rows_of(j), :] = src[rows_of(j), :]
 
     def await_exchange(dst, rsem):
-        await_bytes(dst.at[pl.ds(0, ROWS - CAP), :], rsem)
+        await_bytes(dst.at[pl.ds(0, PIECE - SUB), :], rsem)
+
+    def cut(i):
+        return pl.ds(i * PIECE, PIECE)
 
     def cols(i):
         return pl.ds(i * Q, Q)
@@ -173,23 +187,27 @@
         pick = jnp.where(at[0] | at[1] | at[2] | at[3], 1.0, 0.0).astype(BF)
         block = (za, zb)[chunk][b, pl.ds(0, TOK), :]
         xs[b, chunk] = jnp.dot(pick, block, preferred_element_type=F32).astype(BF)
-        exchange(xs.at[b, chunk], xf.at[b, :, cols(chunk)], x_s.at[b, chunk], x_r.at[b, chunk])
-
-    def spread(b):
-        await_exchange(xf.at[b, :, cols(A)], x_r.at[b, A])
+        for i in range(CUTS):
+            exchange(
+                xs.at[b, chunk, cut(i)], xf.at[b, cut(i), cols(chunk)],
+                x_s.at[b, chunk, i], x_r.at[b, chunk, i],
+            )
+
+    def spread(b, i):
+        await_exchange(xf.at[b, cut(i), cols(A)], x_r.at[b, A, i])
         for side in range(2):
             sends.append(
                 send(
-                    xf.at[b, :, cols(A)], xf.at[b, :, cols(2 + side)],
-                    y_s.at[side, b], y_r.at[side, b], ydev[side],
+                    xf.at[b, cut(i), cols(A)], xf.at[b, cut(i), cols(2 + side)],
+                    y_s.at[side, b, i], y_r.at[side, b, i], ydev[side],
                 )
             )
 
-    def experts(b):
-        await_exchange(xf.at[b, :, cols(B)], x_r.at[b, B])
+    def experts(b, i):
+        await_exchange(xf.at[b, cut(i), cols(B)], x_r.at[b, B, i])
         for side in range(2):
-            await_bytes(xf.at[b, :, cols(2 + side)], y_r.at[side, b])
-        rows = xf[b]
+            await_bytes(xf.at[b, cut(i), cols(2 + side)], y_r.at[side, b, i])
+        rows = xf[b, cut(i), :]
         for n in range(2):
             gate = jnp.dot(rows, wgu[:, pl.ds(n * 256, 256)], preferred_element_type=F32)
             upper = jnp.dot(rows, wgu[:, pl.ds(Q + n * 256, 256)], preferred_element_type=F32)
@@ -198,39 +216,40 @@
             hid[:, pl.ds(n * 256, 256)] = (
                 (upper + 1.0) * (gate * jax.nn.sigmoid(1.702 * gate))
             ).astype(BF)
-        for i in (2, 3, 1, 0):
-            part = jnp.dot(hid[...], wdn[:, cols(i)], preferred_element_type=F32)
-            ps[b, i] = part.astype(BF)
-            if i >= 2:
-                side = 3 - i
+        for q in (2, 3, 1, 0):
+            part = jnp.dot(hid[...], wdn[:, cols(q)], preferred_element_type=F32)
+            ps[b, q, cut(i), :] = part.astype(BF)
+            if q >= 2:
+                side = 3 - q
                 sends.append(
                     send(
-                        ps.at[b, i], yr.at[side, b],
-                        p_s.at[side, b], p_r.at[side, b], ydev[side],
+                        ps.at[b, q, cut(i)], yr.at[side, b, cut(i)],
+                        p_s.at[side, b, i], p_r.at[side, b, i], ydev[side],
                     )
                 )
-            elif i == 1:
-                exchange(ps.at[b, 1], cr.at[b, B], q_s.at[b, B], q_r.at[b, B])
-
-    def give_back(b):
+            elif q == 1:
+                exchange(
+                    ps.at[b, 1, cut(i)], cr.at[b, B, cut(i)], q_s.at[b, B, i], q_r.at[b, B, i]
+                )
+
+    def give_back(b, i):
+        total = ps[b, 0, cut(i), :].astype(F32)
         for side in range(2):
-            await_bytes(yr.at[side, b], p_r.at[side, b])
-        total = ps[b, 0].astype(F32) + yr[0, b].astype(F32) + yr[1, b].astype(F32)
-        xs2[b] = total.astype(BF)
-        exchange(xs2.at[b], cr.at[b, A], q_s.at[b, A], q_r.at[b, A])
-
-    def combine(b):
-        for chunk in (A, B):
-            await_exchange(cr.at[b, chunk], q_r.at[b, chunk])
+            await_bytes(yr.at[side, b, cut(i)], p_r.at[side, b, i])
+            total = total + yr[side, b, cut(i), :].astype(F32)
+        xs2[b, cut(i), :] = total.astype(BF)
+        exchange(xs2.at[b, cut(i)], cr.at[b, A, cut(i)], q_s.at[b, A, i], q_r.at[b, A, i])
+
+    def combine(b, chunk):
+        for i in range(CUTS):
+            await_exchange(cr.at[b, chunk, cut(i)], q_r.at[b, chunk, i])
         info, at = places(b)
         weight = jnp.zeros((ROWS, TOK), F32)
         for k in range(4):
             weight = jnp.where(at[k], info[8 + k : 9 + k], weight)
-        weight = weight.astype(BF)
-        for chunk in (A, B):
-            tsum[b, chunk] = lax.dot_general(
-                weight, cr[b, chunk], (((0,), (0,)), ((), ())), preferred_element_type=F32
-            )
+        tsum[b, chunk] = lax.dot_general(
+            weight.astype(BF), cr[b, chunk], (((0,), (0,)), ((), ())), preferred_element_type=F32
+        )
 
     def span(part):
         return pl.ds(part * (TOK // PARTS), TOK // PARTS)
@@ -264,15 +283,20 @@
         exs[span(part), :] = arrived(B, part).astype(BF)
         sends.append(
             send(
-                exs.at[span(part), :], exr.at[span(part), :],
+                exs.at[span(part), :], far_hbm.at[span(part), :],
                 e_s.at[part], e_r.at[part], (me, y_far),
             )
         )
 
+    results = []
+
     def finish_own(part):
-        own = arrived(A, part)
-        await_bytes(exr.at[span(part), :], e_r.at[part])
-        out_ref[span(part), :] = (own + exr[span(part), :].astype(F32)).astype(BF)
+        own_ref[span(part), :] = arrived(A, part)
+        copy = pltpu.make_async_copy(
+            own_ref.at[span(part), :], own_hbm.at[span(part), :], o_sem.at[part]
+        )
+        copy.start()
+        results.append(copy)
 
     waiting = list(weights)
     for name in SCHEDULE:
@@ -280,39 +304,44 @@
         if name[0] == "F":
             while waiting:
                 waiting.pop().wait()
-        if name[0] in "YFG":
-            arg = arg[:1]
         {
             "Z": z_step, "D": dispatch, "Y": spread, "F": experts, "G": give_back,
             "C": combine, "r": reduce_step, "E": finish_far, "O": finish_own,
         }[name[0]](*arg)
 
+    for part in range(PARTS):
+        await_bytes(far_hbm.at[span(part), :], e_r.at[part])
+    for copy in results:
+        copy.wait()
     for copy in sends:
         copy.wait_send()
     for b in range(NZ):
-        for chunk in (A, B):
-            await_exchange(xs.at[b, chunk], x_s.at[b, chunk])
-        await_exchange(xs2.at[b], q_s.at[b, A])
-        await_exchange(ps.at[b, 1], q_s.at[b, B])
+        for i in range(CUTS):
+            for chunk in (A, B):
+                await_exchange(xs.at[b, chunk, cut(i)], x_s.at[b, chunk, i])
+            await_exchange(xs2.at[b, cut(i)], q_s.at[b, A, i])
+            await_exchange(ps.at[b, 1, cut(i)], q_s.at[b, B, i])
 
 
 def per_device(tokens, norm_gain, expert_ids, route_weights, gate_weight, up_weight, down_weight):
     vmem = pl.BlockSpec(memory_space=pltpu.VMEM)
     hbm = pl.BlockSpec(memory_space=pl.ANY)
     dma = pltpu.SemaphoreType.DMA
-    return pl.pallas_call(
+    own, far = pl.pallas_call(
         kernel,
-        out_shape=jax.ShapeDtypeStruct((TOK, Q), BF),
-        in_specs=[vmem, vmem, vmem, vmem, hbm, hbm, hbm],
-        out_specs=vmem,
+        out_shape=[jax.ShapeDtypeStruct((TOK, Q), F32), jax.ShapeDtypeStruct((TOK, Q), BF)],
+        in_specs=[hbm, vmem, vmem, vmem, hbm, hbm, hbm],
+        out_specs=[hbm, hbm],
         scratch_shapes=[
+            pltpu.VMEM((TOK, W), BF),
+            pltpu.VMEM((TOK, Q), F32),
             pltpu.VMEM((NZ, TOK + META, Q), BF),
             pltpu.VMEM((NZ, TOK, Q), BF),
             pltpu.VMEM((NZ, 2, ROWS, Q), BF),
             pltpu.VMEM((NZ, ROWS, W), BF),
             pltpu.VMEM((W, 2 * Q), BF),
             pltpu.VMEM((Q, W), BF),
-            pltpu.VMEM((ROWS, Q), BF),
+            pltpu.VMEM((PIECE, Q), BF),
             pltpu.VMEM((NZ, 4, ROWS, Q), BF),
             pltpu.VMEM((2, NZ, ROWS, Q), BF),
             pltpu.VMEM((NZ, ROWS, Q), BF),
@@ -321,14 +350,13 @@
             pltpu.VMEM((2, HALF, 2, TOK, Q), BF),
             pltpu.VMEM((2, HALF, 2, TOK, Q), BF),
             pltpu.VMEM((TOK, Q), BF),
-            pltpu.VMEM((TOK, Q), BF),
             pltpu.VMEM((META, TOK), F32),
-            dma((12,)),
+            dma, dma((PARTS,)), dma((12,)),
             dma((2, HALF, 2, PARTS)), dma((2, HALF, 2, PARTS)),
-            dma((NZ, 2)), dma((NZ, 2)),
-            dma((2, NZ)), dma((2, NZ)),
-            dma((2, NZ)), dma((2, NZ)),
-            dma((NZ, 2)), dma((NZ, 2)),
+            dma((NZ, 2, CUTS)), dma((NZ, 2, CUTS)),
+            dma((2, NZ, CUTS)), dma((2, NZ, CUTS)),
+            dma((2, NZ, CUTS)), dma((2, NZ, CUTS)),
+            dma((NZ, 2, CUTS)), dma((NZ, 2, CUTS)),
             dma((2, HALF, 2, PARTS)), dma((2, HALF, 2, PARTS)),
             dma((PARTS,)), dma((PARTS,)),
         ],
@@ -340,6 +368,7 @@
         tokens, norm_gain.reshape(1, W), expert_ids.T, route_weights.T,
         gate_weight, up_weight, down_weight,
     )
+    return (own + far.astype(F32)).astype(BF)
 
 
 def solution(mesh):

time: 132 us -> 125 us (0.947)
  Pallas kernels: 130 us -> 123 us
  other arithmetic: 0 us -> 1.88 us
  local copies, waits for them, and re-layouts: 1.67 us -> 0 us
    pallas_call x1, Pallas kernels: 130 us -> 123 us  [per_device(): pl.pallas_call(kernel, out_shape=[jax.ShapeDtypeStruct((TOK, Q), F32), ja...]
    convert_element_type x0 -> x1, other arithmetic: none -> 1.88 us  [per_device(): return (own + far.astype(F32)).astype(BF)]
    unnamed x1 -> x0, local copies, waits for them, and re-layouts: 1.67 us -> none
where the time goes in v2:
time: 125 us; the launch traced here: 124 us
  Pallas kernels  123 us (98%)
  other arithmetic  1.88 us (2%)
    pallas_call x1, Pallas kernels, per_device(): pl.pallas_call(kernel, out_shape=[jax.ShapeDtypeStruct((TOK, Q), F32), ja...  123 us

profile of v2, /device:TPU:1, one launch (start us, length us, event | category | flops | bytes accessed | tf_op | source)
XLA Modules:
  0.0 124.4 jit_solution(5253028269127216969)
XLA Ops:
  0.0 122.5 %moe.1 = (f32[256,512]{1,0:T(8,128)}, bf16[256,512]{1,0:T(8,128)(2,1)}) custom-call(bf16[256,2048]{1,0:T(8,128)(2,1)} %tok_hbm.1, f32[1,2048]{1,0:T(1,128)} %bitcast.3, s32[4,256]{1,0:T(4,128)} %bitcast.4, f32[4,256]{1,0:T(4,128)} %bitcast.5, bf16[1,2048,512]{2,1,0:T(8,128)(2,1)} %wg_ref.1, bf16[1,2048,512]{2,1,0:T(8,128)(2,1)} %wu_ref.1, ...), custom_call_target="tpu_custom_call" | custom-call | tf_op jit(solution)/shard_map/moe/pallas_call | solution.py:330
  122.5 1.9 %add_convert_fusion = bf16[256,512]{1,0:T(8,128)(2,1)} fusion(f32[256,512]{1,0:T(8,128)} %get-tuple-element.7, bf16[256,512]{1,0:T(8,128)(2,1)} %get-tuple-element.8), kind=kLoop, calls=%fused_computation | loop fusion | flops 393216 | bytes 1048576 | tf_op jit(solution)/shard_map/convert_element_type | solution.py:371

commit v3 on v2

--- a/solution.py
+++ b/solution.py
@@ -22,6 +22,8 @@
 CUTS = 1
 SUB = CAP // CUTS
 PIECE = ROWS // CUTS
+C = Q // PARTS
+EARLY = (0, 1, NZ - 1)
 BF = jnp.bfloat16
 F32 = jnp.float32
 
@@ -31,23 +33,24 @@
 
 
 SCHEDULE = (
-    "D00", "Z1100", "D01", "Z1101", "Z0100", "Z0101", "D70", "Y00", "Z1110", "D10", "Z1111", "Y70",
-    "D11", "Y10", "Z0200", "Z0201", "D60", "Z1201", "Z0300", "Z1200", "Z0110", "D20", "Z1210", "Y60",
-    "Z0301", "D50", "Z0111", "Z1301", "D71", "Y20", "Z1211", "D21", "Z0401", "Z1310", "Z0210", "Z1300",
-    "Z0400", "D40", "Y50", "Z0211", "D30", "Z1311", "D61", "Y40", "Z1410", "Z1411", "Z0310", "Z0311",
-    "D51", "D41", "D31", "Y30", "F50", "F40", "F30", "F20", "F60", "C41", "r1410", "r1411", "C31",
-    "r0311", "G40", "C51", "G50", "r0310", "C21", "F10", "r0211", "r1310", "G30", "C40", "r0210",
-    "r1311", "C61", "r0401", "C50", "r1300", "r0400", "F70", "r1211", "G20", "C11", "r1210", "r1301",
-    "C30", "r0110", "r0301", "G60", "F00", "r0300", "C71", "r1111", "G10", "r0111", "r1110", "C60",
-    "C20", "r0201", "C01", "r0200", "r1201", "G70", "r1200", "C10", "E1", "r0101", "C70", "r1101",
-    "r0100", "E0", "G00", "r1100", "C00", "O1", "O0",
+    "H00", "B11", "H01", "B10", "J00", "Z1100", "Z0100", "H10", "H70", "J01", "Z0101", "H71", "D01",
+    "J10", "Z0200", "Z1101", "J70", "H11", "Z1110", "Z1111", "Z0201", "D60", "D11", "J71", "B00", "B01",
+    "Z1200", "J11", "Z0300", "Z0301", "D50", "Z1201", "Y60", "Z1210", "D20", "Z0111", "Z1211", "Z0110",
+    "D71", "Y50", "Z0400", "Z1300", "D21", "Y20", "Z0401", "D40", "Z1310", "Z1301", "D30", "Z0211",
+    "Z1311", "D31", "Z0210", "D61", "Y40", "Y30", "Z1411", "Z1410", "D41", "F20", "Z0310", "Z0311",
+    "D51", "F40", "F30", "F50", "C41", "r1410", "F60", "C31", "r0310", "r0311", "r1411", "C51", "G40",
+    "r1310", "F70", "C61", "C21", "r1311", "r0210", "G20", "C40", "r0401", "r0400", "r1210", "r0211",
+    "G30", "F10", "G50", "r1211", "C71", "r1110", "C30", "r0300", "G60", "r0301", "C20", "r1111", "F00",
+    "C50", "r1301", "C11", "r0111", "r1300", "G70", "C60", "r0110", "r0200", "r1201", "G10", "C01",
+    "r0201", "r1200", "C70", "E0", "r1101", "E1", "C10", "r0100", "G00", "r1100", "r0101", "C00", "O0",
+    "O1",
 )
 
 
 def kernel(
     tok_hbm, gain_ref, ids_ref, rw_ref, wg_ref, wu_ref, wd_ref, own_hbm, far_hbm,
     tok_ref, own_ref, za, zb, xs, xf, wgu, wdn, hid, ps, yr, xs2, cr, tsum, rin, rout, exs, info_ref,
-    t_sem, o_sem, w_sem, z_s, z_r, x_s, x_r, y_s, y_r, p_s, p_r, q_s, q_r, c_s, c_r, e_s, e_r,
+    t_sem, o_sem, h_s, h_r, j_s, j_r, w_sem, z_s, z_r, x_s, x_r, y_s, y_r, p_s, p_r, q_s, q_r, c_s, c_r, e_s, e_r,
 ):
     me = lax.axis_index("ep")
     y = lax.axis_index("tp")
@@ -67,8 +70,13 @@
     def quarter(i):
         return pl.ds(pl.multiple_of((y, y_far, y_down, y_up)[i] * Q, Q), Q)
 
-    tokens = pltpu.make_async_copy(tok_hbm, tok_ref, t_sem)
-    tokens.start()
+    halves = [pl.ds(i * (TOK // 2), TOK // 2) for i in range(2)]
+    tokens = [
+        pltpu.make_async_copy(tok_hbm.at[rows, :], tok_ref.at[rows, :], t_sem.at[i])
+        for i, rows in enumerate(halves)
+    ]
+    for copy in tokens:
+        copy.start()
 
     barrier = pltpu.get_barrier_semaphore()
     partners = list(zdev) + list(ydev) + [(me, y_far)]
@@ -110,55 +118,59 @@
         slot = jnp.sum(jnp.where(hits[k], before, 0.0), axis=0, keepdims=True)
         info_ref[pl.ds(4 + k, 1), :] = slot
     info_ref[pl.ds(8, 4), :] = rw_ref[...]
-    za[0, pl.ds(TOK, META), pl.ds(0, TOK)] = info_ref[...].astype(BF)
-    za[0, pl.ds(TOK, META), pl.ds(TOK, TOK)] = jnp.zeros((META, TOK), BF)
-
-    tokens.wait()
-    for copy in weights:
-        copy.start()
-    values = tok_ref[...].astype(F32)
-    scale = lax.rsqrt(jnp.mean(values * values, axis=1, keepdims=True) + 1e-06)
-    for i, buf in enumerate((za, zb)):
-        part = tok_ref[:, quarter(i)].astype(F32) * scale * gain_ref[:, quarter(i)]
-        buf[0, pl.ds(0, TOK), :] = part.astype(BF)
-
-    pl.semaphore_wait(barrier, len(partners))
-
-    def piece(chunk, part):
-        size = (TOK + META, TOK)[chunk]
-        step = TOK // PARTS
-        first = size - TOK
-        return pl.ds(0, step + first) if part == 0 else pl.ds(first + part * step, step)
+    za[0, 0, pl.ds(TOK, META), :] = info_ref[...].astype(BF)
+
+    def piece(chunk, b, part):
+        rows = TOK + META if (chunk, part) == (A, 0) else TOK
+        return (za, zb)[chunk].at[b, part, pl.ds(0, rows), :]
 
     def z_send(direction, hop, chunk, part):
-        buf = (za, zb)[chunk]
         here = (-hop if direction == R else hop) % NZ
         there = (-(hop + 1) if direction == R else hop + 1) % NZ
-        rows = piece(chunk, part)
         sends.append(
             send(
-                buf.at[here, rows], buf.at[there, rows],
+                piece(chunk, here, part), piece(chunk, there, part),
                 z_s.at[direction, hop, chunk, part], z_r.at[direction, hop, chunk, part],
                 zdev[direction],
             )
         )
 
     def z_step(direction, hop, chunk, part):
-        buf = (za, zb)[chunk]
         slot = (-hop if direction == R else hop) % NZ
-        await_bytes(buf.at[slot, piece(chunk, part)], z_r.at[direction, hop - 1, chunk, part])
+        await_bytes(piece(chunk, slot, part), z_r.at[direction, hop - 1, chunk, part])
         if hop < top_hop(direction, chunk):
             z_send(direction, hop, chunk, part)
 
-    for chunk in (A, B):
-        for part in range(PARTS):
-            for direction in (R, L):
-                z_send(direction, 0, chunk, part)
+    def normalise(chunk, part):
+        at = (y, y_far)[chunk] * Q + part * C
+        cols = pl.ds(pl.multiple_of(at, C), C)
+        for rows, scale in zip(halves, scales):
+            value = tok_ref[rows, cols].astype(F32) * scale * gain_ref[:, cols]
+            (za, zb)[chunk][0, part, rows, :] = value.astype(BF)
+
+    scales = []
+    for copy, rows in zip(tokens, halves):
+        copy.wait()
+        values = tok_ref[rows, :].astype(F32)
+        scales.append(lax.rsqrt(jnp.mean(values * values, axis=1, keepdims=True) + 1e-06))
+    for part in range(PARTS):
+        normalise(A, part)
+        if part == 0:
+            pl.semaphore_wait(barrier, len(partners))
+        for direction in (R, L):
+            z_send(direction, 0, A, part)
+    for copy in weights:
+        copy.start()
+    for part in range(PARTS):
+        normalise(B, part)
+
+    def z_start(direction, part):
+        z_send(direction, 0, B, part)
 
     base = (z * ROWS).astype(F32)
 
     def places(b):
-        info = za[b, pl.ds(TOK, META), pl.ds(0, TOK)].astype(F32)
+        info = za[b, 0, pl.ds(TOK, META), :].astype(F32)
         row = lax.broadcasted_iota(jnp.int32, (ROWS, TOK), 0)
         row = lax.rem(row, PIECE) // SUB * CAP + row // PIECE * SUB + lax.rem(row, SUB)
         at = row.astype(F32) + base
@@ -182,31 +194,61 @@
     def cols(i):
         return pl.ds(i * Q, Q)
 
-    def dispatch(b, chunk):
+    def picked(b, chunk, parts):
         info, at = places(b)
         pick = jnp.where(at[0] | at[1] | at[2] | at[3], 1.0, 0.0).astype(BF)
-        block = (za, zb)[chunk][b, pl.ds(0, TOK), :]
-        xs[b, chunk] = jnp.dot(pick, block, preferred_element_type=F32).astype(BF)
-        for i in range(CUTS):
-            exchange(
-                xs.at[b, chunk, cut(i)], xf.at[b, cut(i), cols(chunk)],
-                x_s.at[b, chunk, i], x_r.at[b, chunk, i],
-            )
+        for part in parts:
+            block = (za, zb)[chunk][b, part, pl.ds(0, TOK), :]
+            xs[b, chunk, :, fine(part)] = jnp.dot(
+                pick, block, preferred_element_type=F32
+            ).astype(BF)
+
+    def fine(part):
+        return pl.ds(part * C, C)
+
+    def dispatch(b, chunk):
+        picked(b, chunk, range(PARTS))
+        exchange(
+            xs.at[b, chunk], xf.at[b, :, cols(chunk)], x_s.at[b, chunk, 0], x_r.at[b, chunk, 0]
+        )
+
+    def early_dispatch(b, part):
+        picked(b, A, (part,))
+        exchange(
+            xs.at[b, A, :, fine(part)], xf.at[b, :, fine(part)], h_s.at[b, part], h_r.at[b, part]
+        )
 
     def spread(b, i):
-        await_exchange(xf.at[b, cut(i), cols(A)], x_r.at[b, A, i])
+        await_exchange(xf.at[b, :, cols(A)], x_r.at[b, A, i])
         for side in range(2):
             sends.append(
                 send(
-                    xf.at[b, cut(i), cols(A)], xf.at[b, cut(i), cols(2 + side)],
+                    xf.at[b, :, cols(A)], xf.at[b, :, cols(2 + side)],
                     y_s.at[side, b, i], y_r.at[side, b, i], ydev[side],
                 )
             )
 
+    def early_landing(b, side, part):
+        return xf.at[b, :, pl.ds((2 + side) * Q + part * C, C)]
+
+    def early_spread(b, part):
+        await_exchange(xf.at[b, :, fine(part)], h_r.at[b, part])
+        for side in range(2):
+            sends.append(
+                send(
+                    xf.at[b, :, fine(part)], early_landing(b, side, part),
+                    j_s.at[side, b, part], j_r.at[side, b, part], ydev[side],
+                )
+            )
+
     def experts(b, i):
         await_exchange(xf.at[b, cut(i), cols(B)], x_r.at[b, B, i])
         for side in range(2):
-            await_bytes(xf.at[b, cut(i), cols(2 + side)], y_r.at[side, b, i])
+            if b in EARLY:
+                for part in range(PARTS):
+                    await_bytes(early_landing(b, side, part), j_r.at[side, b, part])
+            else:
+                await_bytes(xf.at[b, cut(i), cols(2 + side)], y_r.at[side, b, i])
         rows = xf[b, cut(i), :]
         for n in range(2):
             gate = jnp.dot(rows, wgu[:, pl.ds(n * 256, 256)], preferred_element_type=F32)
@@ -306,7 +348,7 @@
                 waiting.pop().wait()
         {
             "Z": z_step, "D": dispatch, "Y": spread, "F": experts, "G": give_back,
-            "C": combine, "r": reduce_step, "E": finish_far, "O": finish_own,
+            "C": combine, "r": reduce_step, "B": z_start, "H": early_dispatch, "J": early_spread, "E": finish_far, "O": finish_own,
         }[name[0]](*arg)
 
     for part in range(PARTS):
@@ -317,8 +359,12 @@
         copy.wait_send()
     for b in range(NZ):
         for i in range(CUTS):
-            for chunk in (A, B):
-                await_exchange(xs.at[b, chunk, cut(i)], x_s.at[b, chunk, i])
+            if b in EARLY:
+                for part in range(PARTS):
+                    await_exchange(xs.at[b, A, :, fine(part)], h_s.at[b, part])
+            else:
+                await_exchange(xs.at[b, A], x_s.at[b, A, i])
+            await_exchange(xs.at[b, B], x_s.at[b, B, i])
             await_exchange(xs2.at[b, cut(i)], q_s.at[b, A, i])
             await_exchange(ps.at[b, 1, cut(i)], q_s.at[b, B, i])
 
@@ -335,8 +381,8 @@
         scratch_shapes=[
             pltpu.VMEM((TOK, W), BF),
             pltpu.VMEM((TOK, Q), F32),
-            pltpu.VMEM((NZ, TOK + META, Q), BF),
-            pltpu.VMEM((NZ, TOK, Q), BF),
+            pltpu.VMEM((NZ, PARTS, TOK + META, C), BF),
+            pltpu.VMEM((NZ, PARTS, TOK, C), BF),
             pltpu.VMEM((NZ, 2, ROWS, Q), BF),
             pltpu.VMEM((NZ, ROWS, W), BF),
             pltpu.VMEM((W, 2 * Q), BF),
@@ -351,7 +397,10 @@
             pltpu.VMEM((2, HALF, 2, TOK, Q), BF),
             pltpu.VMEM((TOK, Q), BF),
             pltpu.VMEM((META, TOK), F32),
-            dma, dma((PARTS,)), dma((12,)),
+            dma((2,)), dma((PARTS,)),
+            dma((NZ, PARTS)), dma((NZ, PARTS)),
+            dma((2, NZ, PARTS)), dma((2, NZ, PARTS)),
+            dma((12,)),
             dma((2, HALF, 2, PARTS)), dma((2, HALF, 2, PARTS)),
             dma((NZ, 2, CUTS)), dma((NZ, 2, CUTS)),
             dma((2, NZ, CUTS)), dma((2, NZ, CUTS)),

time: 125 us -> 122 us (0.976)
  Pallas kernels: 123 us -> 120 us
    pallas_call x1, Pallas kernels: 123 us -> 120 us  [per_device(): pl.pallas_call(kernel, out_shape=[jax.ShapeDtypeStruct((TOK, Q), F32), ja...]
where the time goes in v3:
time: 122 us
  Pallas kernels  120 us (98%)
  other arithmetic  1.88 us (2%)
    pallas_call x1, Pallas kernels, per_device(): pl.pallas_call(kernel, out_shape=[jax.ShapeDtypeStruct((TOK, Q), F32), ja...  120 us

profile of v3, /device:TPU:1, one launch (start us, length us, event | category | flops | bytes accessed | tf_op | source)
XLA Modules:
  0.0 121.6 jit_solution(8124499785358895603)
XLA Ops:
  0.0 119.7 %moe.1 = (f32[256,512]{1,0:T(8,128)}, bf16[256,512]{1,0:T(8,128)(2,1)}) custom-call(bf16[256,2048]{1,0:T(8,128)(2,1)} %tok_hbm.1, f32[1,2048]{1,0:T(1,128)} %bitcast.3, s32[4,256]{1,0:T(4,128)} %bitcast.4, f32[4,256]{1,0:T(4,128)} %bitcast.5, bf16[1,2048,512]{2,1,0:T(8,128)(2,1)} %wg_ref.1, bf16[1,2048,512]{2,1,0:T(8,128)(2,1)} %wu_ref.1, ...), custom_call_target="tpu_custom_call" | custom-call | tf_op jit(solution)/shard_map/moe/pallas_call | solution.py:376
  119.7 1.9 %add_convert_fusion = bf16[256,512]{1,0:T(8,128)(2,1)} fusion(f32[256,512]{1,0:T(8,128)} %get-tuple-element.7, bf16[256,512]{1,0:T(8,128)(2,1)} %get-tuple-element.8), kind=kLoop, calls=%fused_computation | loop fusion | flops 393216 | bytes 1048576 | tf_op jit(solution)/shard_map/convert_element_type | solution.py:420

commit v4 on v3

--- a/solution.py
+++ b/solution.py
@@ -180,7 +180,7 @@
         return pl.ds(pl.multiple_of(p * SUB, SUB), SUB)
 
     def exchange(src, dst, ssem, rsem):
-        for o in range(1, NJ):
+        for o in (4, 5, 3, 6, 2, 7, 1):
             p = peer(o)
             send(src.at[rows_of(p), :], dst.at[rows_of(j), :], ssem, rsem, (z * NJ + p, y))
         dst[rows_of(j), :] = src[rows_of(j), :]

time: 122 us -> 121 us (level)
  no operation moved by 1% of the time
where the time goes in v4:
time: 121 us
  Pallas kernels  119 us (98%)
  other arithmetic  1.88 us (2%)
    pallas_call x1, Pallas kernels, per_device(): pl.pallas_call(kernel, out_shape=[jax.ShapeDtypeStruct((TOK, Q), F32), ja...  119 us

profile of v4, /device:TPU:1, one launch (start us, length us, event | category | flops | bytes accessed | tf_op | source)
XLA Modules:
  0.0 120.6 jit_solution(1404870386270678970)
XLA Ops:
  0.0 118.7 %moe.1 = (f32[256,512]{1,0:T(8,128)}, bf16[256,512]{1,0:T(8,128)(2,1)}) custom-call(bf16[256,2048]{1,0:T(8,128)(2,1)} %tok_hbm.1, f32[1,2048]{1,0:T(1,128)} %bitcast.3, s32[4,256]{1,0:T(4,128)} %bitcast.4, f32[4,256]{1,0:T(4,128)} %bitcast.5, bf16[1,2048,512]{2,1,0:T(8,128)(2,1)} %wg_ref.1, bf16[1,2048,512]{2,1,0:T(8,128)(2,1)} %wu_ref.1, ...), custom_call_target="tpu_custom_call" | custom-call | tf_op jit(solution)/shard_map/moe/pallas_call | solution.py:376
  118.8 1.9 %add_convert_fusion = bf16[256,512]{1,0:T(8,128)(2,1)} fusion(f32[256,512]{1,0:T(8,128)} %get-tuple-element.7, bf16[256,512]{1,0:T(8,128)(2,1)} %get-tuple-element.8), kind=kLoop, calls=%fused_computation | loop fusion | flops 393216 | bytes 1048576 | tf_op jit(solution)/shard_map/convert_element_type | solution.py:420
